TPU v7x, 32 devices: a whole 2x2x4 slice. The times are simulated.
32 devices in a mesh: sp: 16 (over z, y, x), tp: 2 (over core).
Axes of the slice: x: 2, y: 2, z: 4, core: 2. Of those that a mesh axis runs over, the one named last changes fastest.
Arguments:
- acceptor_signal: bfloat16 [2048, 1024], P('sp', 'tp'), may hold values from -6 to 6
- address_entries: bfloat16 [2048, 1024], P('sp', 'tp'), may hold values from -6 to 6
- payload_entries: bfloat16 [2048, 1024], P('sp', 'tp'), may hold values from -6 to 6
- fading_logits: float32 [2048, 1024], P('sp', 'tp'), may hold values from -12 to -2
- learning_rate_logits: float32 [2048, 1024], P('sp', 'tp'), may hold values from -10 to 4
- exit_switch_entries: bfloat16 [2048, 1024], P('sp', 'tp'), may hold values from -6 to 6
- extra_reward_weights: float32 [1024], P('tp'), may hold values from -0.3 to 0.3
- subspace_rescale_weights: float32 [1024], P('tp'), may hold values from 0.1 to 1.9
- timemix_exit_weights: bfloat16 [1024, 2048], P('tp'), may hold values from -0.1875 to 0.1875
- skip_stream_arriving: bfloat16 [2048, 2048], P(('sp', 'tp')), may hold values from -6 to 6
- pointwise_block_scaling: float32 [2048], replicated, may hold values from 0.1 to 1.9
- switch_projection: bfloat16 [2048, 5632], P('sp', 'tp'), may hold values from -0.125 to 0.125
- widening_projection: bfloat16 [2048, 5632], P('sp', 'tp'), may hold values from -0.125 to 0.125
- switch_filter_coefficients: float32 [3, 5632], P(None, 'tp'), may hold values from -3.5 to 3.5
- narrowing_projection: bfloat16 [5632, 2048], P('tp', 'sp'), may hold values from -0.078125 to 0.078125
Outputs:
- layer_out: bfloat16 [2048, 2048], P(('sp', 'tp'))
All inputs are finite; a program needn't handle non-finite values.
Results may differ from a plain program's by a relative error of at most 0.019.
Values may be sent and summed in bfloat16 or wider, within the bound.
A program may use at most 128 MiB of HBM per device.

v0:
```python
import jax
import jax.numpy as jnp
from jax import lax
from jax.sharding import PartitionSpec as P

SUBSPACE_WIDTH = 64
SPAN = 16
group_eps = 0.00064
norm_eps = 1e-06
highest = lax.Precision.HIGHEST


def carried_in(shard, axis, join, neutral):
    place = lax.axis_index(axis)
    gathered = jax.tree.map(
        lambda a, kind: lax.all_gather(a.astype(kind), axis), shard, (jnp.bfloat16, jnp.bfloat16)
    )
    state = jax.tree.map(lambda a, e: jnp.zeros_like(a) + jnp.asarray(e, a.dtype), shard, neutral)

    def one(lap, state):
        return join(
            state,
            jax.tree.map(
                lambda a, own: lax.dynamic_index_in_dim(a, lap, 0, False).astype(own.dtype),
                gathered,
                shard,
            ),
        )

    return lax.fori_loop(0, place, one, state)


def shifted(block, axis, distance):
    devices = range(lax.axis_size(axis))
    route = [(i - distance, i) for i in devices if i - distance in devices]
    return lax.ppermute(block, axis, route)


def by_heads(array):
    return array.astype(jnp.float32).reshape(array.shape[0], -1, SUBSPACE_WIDTH)


def mechanism_inputs(
    acceptor_signal, address_entries, payload_entries, fading_logits, learning_rate_logits
):
    acceptor_entries = by_heads(acceptor_signal)
    address_mapped = by_heads(address_entries)
    payload_mapped = by_heads(payload_entries)
    log_rate = -jax.nn.softplus(-fading_logits) - 0.5
    fading = by_heads(jnp.exp(-jnp.exp(log_rate)))
    erase_rate = by_heads(jax.nn.sigmoid(learning_rate_logits))
    length = jnp.sqrt(jnp.sum(address_mapped * address_mapped, axis=-1, keepdims=True))
    unit_key = address_mapped / jnp.maximum(length, 1.0)
    return (
        acceptor_entries,
        address_mapped,
        payload_mapped,
        fading,
        -unit_key,
        unit_key * erase_rate,
    )


def subspace_outcomes(
    acceptor_entries,
    address_mapped,
    payload_mapped,
    closing_memory,
    subspace_rescale_weights,
    extra_reward_weights,
    exit_switch_entries,
):
    centred = closing_memory - jnp.mean(closing_memory, axis=-1, keepdims=True)
    rescaled_arguments = centred * lax.rsqrt(
        jnp.mean(centred * centred, axis=-1, keepdims=True) + group_eps
    )
    scaling_fetch = subspace_rescale_weights.reshape(-1, SUBSPACE_WIDTH)
    extra_reward_fetch = extra_reward_weights.reshape(-1, SUBSPACE_WIDTH)
    present_extra_reward = (
        jnp.sum(acceptor_entries * address_mapped * extra_reward_fetch, axis=-1, keepdims=True)
        * payload_mapped
    )
    timemix_product = rescaled_arguments * scaling_fetch + present_extra_reward
    timemix_product = timemix_product.reshape(
        timemix_product.shape[0], -1
    ) * exit_switch_entries.astype(jnp.float32)
    return timemix_product.astype(jnp.bfloat16)


def compose(earlier, latter):
    mapping = jnp.einsum("...ij,...jk->...ik", earlier[0], latter[0], precision=highest)
    state = jnp.einsum("...ij,...jk->...ik", earlier[1], latter[0], precision=highest) + latter[1]
    return (mapping, state)


def span_step(carried, sublevel_arguments):
    state, mapping = carried
    acceptor_entries, address_mapped, payload_mapped, fading, erase_dir, erase_amt = (
        sublevel_arguments
    )
    along = jnp.einsum("bhij,bhj->bhi", state, erase_dir, precision=highest)
    map_along = jnp.einsum("bhij,bhj->bhi", mapping, erase_dir, precision=highest)
    state = (
        state * fading[:, :, None, :]
        + along[..., None] * erase_amt[:, :, None, :]
        + payload_mapped[..., None] * address_mapped[:, :, None, :]
    )
    mapping = mapping * fading[:, :, None, :] + map_along[..., None] * erase_amt[:, :, None, :]
    local_out = jnp.einsum("bhij,bhj->bhi", state, acceptor_entries, precision=highest)
    probe = jnp.einsum("bhij,bhj->bhi", mapping, acceptor_entries, precision=highest)
    return ((state, mapping), (local_out, probe))


def recurrence(sublevel_arguments):
    token_count, head_count = (sublevel_arguments[0].shape[0], sublevel_arguments[0].shape[1])
    blocks = token_count // SPAN

    def arrange(member):
        return jnp.moveaxis(member.reshape(blocks, SPAN, head_count, SUBSPACE_WIDTH), 1, 0)

    arranged = tuple((arrange(member) for member in sublevel_arguments))
    unit_map = jnp.eye(SUBSPACE_WIDTH, dtype=jnp.float32)
    zero_state = jnp.zeros((blocks, head_count, SUBSPACE_WIDTH, SUBSPACE_WIDTH), jnp.float32)
    start_maps = jnp.broadcast_to(unit_map, zero_state.shape)
    (block_states, block_maps), (local_out, probe) = lax.scan(
        span_step, (zero_state, start_maps), arranged
    )
    cum_maps, cum_states = lax.associative_scan(compose, (block_maps, block_states))
    head_unit = jnp.broadcast_to(unit_map, (head_count, SUBSPACE_WIDTH, SUBSPACE_WIDTH))
    head_zero = jnp.zeros((head_count, SUBSPACE_WIDTH, SUBSPACE_WIDTH), jnp.float32)
    _, incoming = carried_in((cum_maps[-1], cum_states[-1]), "sp", compose, (head_unit, head_zero))
    prior_maps = jnp.concatenate([head_unit[None], cum_maps[:-1]], axis=0)
    prior_states = jnp.concatenate([head_zero[None], cum_states[:-1]], axis=0)
    entry = jnp.einsum("hij,bhjk->bhik", incoming, prior_maps, precision=highest) + prior_states
    closing_memory = local_out + jnp.einsum("bhij,tbhj->tbhi", entry, probe, precision=highest)
    return jnp.moveaxis(closing_memory, 0, 1).reshape(token_count, head_count, SUBSPACE_WIDTH)


def body(
    acceptor_signal,
    address_entries,
    payload_entries,
    fading_logits,
    learning_rate_logits,
    exit_switch_entries,
    extra_reward_weights,
    subspace_rescale_weights,
    timemix_exit_weights,
    skip_stream_arriving,
    pointwise_block_scaling,
    switch_projection,
    widening_projection,
    switch_filter_coefficients,
    narrowing_projection,
):
    gate_full, up_full, down_full = (
        lax.all_gather(switch_projection, "sp", axis=0, tiled=True),
        lax.all_gather(widening_projection, "sp", axis=0, tiled=True),
        lax.all_gather(narrowing_projection, "sp", axis=1, tiled=True),
    )
    sublevel_arguments = mechanism_inputs(
        acceptor_signal, address_entries, payload_entries, fading_logits, learning_rate_logits
    )
    closing_memory = recurrence(sublevel_arguments)
    timemix_product = subspace_outcomes(
        sublevel_arguments[0],
        sublevel_arguments[1],
        sublevel_arguments[2],
        closing_memory,
        subspace_rescale_weights,
        extra_reward_weights,
        exit_switch_entries,
    )
    token_count = timemix_product.shape[0]
    picked = timemix_product
    attended = lax.psum_scatter(
        jnp.dot(picked, timemix_exit_weights, preferred_element_type=jnp.float32).astype(
            jnp.bfloat16
        ),
        "tp",
        scatter_dimension=0,
        tiled=True,
    ).astype(jnp.float32)
    hidden_res = skip_stream_arriving.astype(jnp.float32) + attended
    rescaled_arguments = (
        hidden_res
        * lax.rsqrt(jnp.mean(hidden_res * hidden_res, axis=-1, keepdims=True) + norm_eps)
        * pointwise_block_scaling
    )
    rescaled_arguments = rescaled_arguments.astype(jnp.bfloat16)
    all_rows = lax.all_gather(rescaled_arguments, "tp", axis=0, tiled=True)
    gate_acc = jnp.dot(all_rows, gate_full, preferred_element_type=jnp.float32)
    up_acc = jnp.dot(all_rows, up_full, preferred_element_type=jnp.float32)
    gate_pre = gate_acc.astype(jnp.bfloat16)
    up_part = up_acc.astype(jnp.bfloat16)
    taps = switch_filter_coefficients.shape[0]
    tail_rows = shifted(gate_pre[token_count - taps + 1 :], "sp", 1)
    extended = jnp.concatenate([tail_rows, gate_pre], axis=0).astype(jnp.float32)
    conv_out = jnp.zeros(gate_pre.shape, jnp.float32)
    for tap in range(taps):
        conv_out = conv_out + switch_filter_coefficients[tap] * extended[tap : tap + token_count]
    hidden = (jax.nn.silu(conv_out) * up_part.astype(jnp.float32)).astype(jnp.bfloat16)
    picked = hidden
    projected = lax.psum_scatter(
        jnp.dot(picked, down_full, preferred_element_type=jnp.float32).astype(jnp.bfloat16),
        "tp",
        scatter_dimension=0,
        tiled=True,
    ).astype(jnp.float32)
    return (hidden_res + projected).astype(jnp.bfloat16)


def solution(mesh):
    return jax.shard_map(
        body,
        mesh=mesh,
        in_specs=(
            P("sp", "tp"),
            P("sp", "tp"),
            P("sp", "tp"),
            P("sp", "tp"),
            P("sp", "tp"),
            P("sp", "tp"),
            P("tp"),
            P("tp"),
            P("tp", None),
            P(("sp", "tp"), None),
            P(),
            P("sp", "tp"),
            P("sp", "tp"),
            P(None, "tp"),
            P("tp", "sp"),
        ),
        out_specs=P(("sp", "tp"), None),
        check_vma=False,
    )
```

profile of v0, /device:TPU:0, one launch (start us, length us, event | category | flops | bytes accessed | tf_op | source)
XLA Modules:
  0.0 1192.7 jit_solution(1004884859613980477)
XLA Ops:
  23.3 418.0 %while.30 = (s32[]{:T(128)}, f32[8,8,64,64]{3,2,1,0:T(8,128)}, f32[8,8,64,64]{3,2,1,0:T(8,128)}, f32[16,8,8,64]{3,0,2,1:T(8,128)}, f32[16,8,8,64]{3,0,2,1:T(8,12...) while((s32[]{:T(128)}, f32[8,8,64,64]{3,2,1,0:T(8,128)}, ...), condition=%wide.region_2.3_spmd.clone, body=%wide.region_1.2_spmd.clone.sunk | while | flops 15204355 | bytes 25657612 | solution.py:125
  41.1 4.9 convolution_bitcast_fusion.9
  48.5 5.1 fusion.113
  67.3 4.9 convolution_bitcast_fusion.9
  74.8 5.1 fusion.113
  93.5 4.9 convolution_bitcast_fusion.9
  101.0 5.1 fusion.113
  106.1 3.4 fusion.112
  119.7 4.9 convolution_bitcast_fusion.9
  127.2 5.1 fusion.113
  132.3 3.4 fusion.112
  146.0 4.9 convolution_bitcast_fusion.9
  153.4 5.1 fusion.113
  158.5 3.4 fusion.112
  172.2 4.9 convolution_bitcast_fusion.9
  179.7 5.1 fusion.113
  184.8 3.4 fusion.112
  198.4 4.9 convolution_bitcast_fusion.9
  205.9 5.1 fusion.113
  211.0 3.4 fusion.112
  224.6 4.9 convolution_bitcast_fusion.9
  232.1 5.1 fusion.113
  237.2 3.4 fusion.112
  250.9 4.9 convolution_bitcast_fusion.9
  258.4 5.1 fusion.113
  263.5 3.4 fusion.112
  277.1 4.9 convolution_bitcast_fusion.9
  284.6 5.1 fusion.113
  289.7 3.4 fusion.112
  303.3 4.9 convolution_bitcast_fusion.9
  310.8 5.1 fusion.113
  315.9 3.4 fusion.112
  329.6 4.9 convolution_bitcast_fusion.9
  337.1 5.1 fusion.113
  342.2 3.4 fusion.112
  355.8 4.9 convolution_bitcast_fusion.9
  363.3 5.1 fusion.113
  382.1 4.9 convolution_bitcast_fusion.9
  389.6 5.1 fusion.113
  408.3 4.9 convolution_bitcast_fusion.9
  415.8 5.1 fusion.113
  434.5 4.9 convolution_bitcast_fusion.9
  452.4 9.2 pad.48
  463.5 9.2 pad.47
  478.5 16.6 %pad.50 = f32[8,8,64,64]{3,2,1,0:T(8,128)} pad(f32[4,8,64,64]{3,2,1,0:T(8,128)} %copy-done.6, f32[]{:T(128)} %constant.54.clone.1), padding=1_0_1x0_0_0x0_0_0x0_0_0 | pad | bytes 1572868 | tf_op jit(solution)/shard_map/pad | solution.py:128
  497.4 16.7 %pad.49 = f32[8,8,64,64]{3,2,1,0:T(8,128)} pad(f32[4,8,64,64]{3,2,1,0:T(8,128)} %pad_maximum_fusion.1, f32[]{:T(128)} %constant.54.clone.1), padding=0_1_1x0_0_0x0_0_0x0_0_0 | pad | bytes 1572868 | tf_op jit(solution)/shard_map/pad | solution.py:128
  518.8 5.9 pad.41
  525.8 5.9 pad.42
  533.4 11.1 pad.112
  546.2 16.6 %pad.67 = f32[7,8,64,64]{3,2,1,0:T(8,128)} pad(f32[4,8,64,64]{3,2,1,0:T(8,128)} %pad_maximum_fusion.1, f32[]{:T(128)} %constant.54.clone.1), padding=0_0_1x0_0_0x0_0_0x0_0_0 | pad | bytes 1441796 | tf_op jit(solution)/shard_map/slice | solution.py:133
  563.8 11.2 pad.44
  577.1 11.2 pad.43
  589.4 3.9 slice_add_fusion.1
  594.9 46.1 %all-gather.6.cloned.1.call-done = bf16[16,8,64,64]{3,2,1,0:T(8,128)(2,1)} async-done(((bf16[1,8,64,64]{3,2,1,0:T(8,128)(2,1)}), bf16[16,8,64,64]{3,2,1,0:T(8,128)(2,1)}) %all-gather.6.cloned.1.call-update) | async-done | bytes 1048592 | tf_op jit(solution)/shard_map/all_gather | solution.py:16
  641.9 3.7 fusion.13
  645.6 3.4 fusion.69
  654.4 39.6 %reduce-scatter.3.cloned.1.call-done = bf16[64,2048]{1,0:T(8,128)(2,1)} async-done(((bf16[128,2048]{1,0:T(8,128)(2,1)}), bf16[64,2048]{1,0:T(8,128)(2,1)}) %reduce-scatter.3.cloned.1.call-update) | async-done | bytes 262160 | tf_op jit(solution)/shard_map/reduce_scatter | solution.py:176
  698.4 140.8 %all-gather.10.cloned.1.call-done = bf16[2048,2816]{1,0:T(8,128)(2,1)} async-done(((bf16[128,2816]{1,0:T(8,128)(2,1)}), bf16[2048,2816]{1,0:T(8,128)(2,1)}) %all-gather.10.cloned.1.call-update) | async-done | bytes 11534352 | tf_op jit(solution)/shard_map/all_gather | solution.py:157
  839.1 6.0 convolution_convert_fusion.1
  845.1 3.4 collective-permute-start
  851.0 130.4 %all-gather.12.cloned.1.call-done = bf16[2048,2816]{1,0:T(8,128)(2,1)} async-done(((bf16[128,2816]{1,0:T(8,128)(2,1)}), bf16[2048,2816]{1,0:T(8,128)(2,1)}) %all-gather.12.cloned.1.call-update) | async-done | bytes 11534352 | tf_op jit(solution)/shard_map/all_gather | solution.py:158
  981.4 182.8 %all-gather.14.cloned.1.call-done = bf16[2816,2048]{1,0:T(8,128)(2,1)} async-done(((bf16[2816,128]{1,0:T(8,128)(2,1)}), bf16[2816,2048]{1,0:T(8,128)(2,1)}) %all-gather.14.cloned.1.call-update) | async-done | bytes 11534352 | tf_op jit(solution)/shard_map/all_gather | solution.py:159
  1164.2 13.6 %convolution_convert_fusion.2 = bf16[128,2048]{1,0:T(8,128)(2,1)} fusion(bf16[2816,2048]{1,0:T(8,128)(2,1)} %all-gather.14.cloned.1.call-done, bf16[128,2048]{1,0:T(8,128)(2,1)S(1)} %all_gather.22, bf16[2048,2816]{1,0:T(8,128)(2,1)} %all-gather.12.cloned.1.call-done, f32[130,2816]{1,0:T(8,128)} %maximum_convert_fusion, f32[2816]{0:T(1024)S(1)} %get-tuple-element.188, ...), kind=kOutput, calls=%fused_computation.27 | convolution fusion | flops 2957737984 | bytes 28476416 | tf_op jit(solution)/shard_map/dot_general | solution.py:205
  1177.8 6.3 reduce-scatter.5.cloned.1.call-done
  (386 shorter events, 295.1 us)
Async XLA Ops:
  6.5 643.8 %copy-start = (bf16[512,2048]{1,0:T(8,128)(2,1)S(1)}, bf16[512,2048]{1,0:T(8,128)(2,1)}, u32[]{:S(2)}) copy-start(bf16[512,2048]{1,0:T(8,128)(2,1)} %param.27) | copy-start | bytes 6291460
  6.5 588.4 %all-gather.8.cloned.1.call-start = ((), (), s32[]{:S(2)}) async-start(), calls=%async_computation.3 | async-start | bytes 2228224 | tf_op jit(solution)/shard_map/all_gather | solution.py:16
  7.9 13.7 %copy-start.21 = (f32[64,64]{1,0:T(8,128)}, f32[64,64]{1,0:T(8,128)S(1)}, u32[]{:S(2)}) copy-start(f32[64,64]{1,0:T(8,128)S(1)} %fusion.61) | copy-start | bytes 49156
  12.0 9.6 copy-start.15
  24.1 8.3 copy-start.4
  34.5 4.7 copy-start.5
  48.5 5.1 copy-start.1
  48.5 10.0 copy-start.4
  60.8 4.7 copy-start.5
  74.8 5.1 copy-start.1
  74.8 10.0 copy-start.4
  101.0 5.1 copy-start.1
  101.0 10.0 copy-start.4
  127.2 5.1 copy-start.1
  127.2 10.0 copy-start.4
  139.4 4.7 copy-start.5
  153.4 5.1 copy-start.1
  153.4 10.0 copy-start.4
  165.6 4.7 copy-start.5
  179.6 5.1 copy-start.1
  179.6 10.0 copy-start.4
  191.9 4.7 copy-start.5
  205.9 5.1 copy-start.1
  205.9 10.0 copy-start.4
  218.1 4.7 copy-start.5
  232.1 5.1 copy-start.1
  232.1 10.0 copy-start.4
  244.3 4.7 copy-start.5
  258.3 5.1 copy-start.1
  258.3 10.0 copy-start.4
  270.6 4.7 copy-start.5
  284.6 5.1 copy-start.1
  284.6 10.0 copy-start.4
  296.8 4.7 copy-start.5
  310.8 5.1 copy-start.1
  310.8 10.0 copy-start.4
  323.0 4.7 copy-start.5
  337.1 5.1 copy-start.1
  337.1 10.0 copy-start.4
  349.3 4.7 copy-start.5
  363.3 5.1 copy-start.1
  363.3 10.0 copy-start.4
  375.5 4.7 copy-start.5
  389.5 5.1 copy-start.1
  389.5 10.0 copy-start.4
  401.8 4.7 copy-start.5
  415.8 5.1 copy-start.1
  415.8 10.0 copy-start.4
  428.0 4.7 copy-start.5
  450.7 10.9 slice-start
  478.5 16.6 %copy-start.17 = (f32[1,8,64,64]{3,2,1,0:T(8,128)S(1)}, f32[1,8,64,64]{3,2,1,0:T(8,128)}, u32[]{:S(2)}) copy-start(f32[1,8,64,64]{3,2,1,0:T(8,128)} %slice.129) | copy-start | bytes 393220
  515.8 125.2 %all-gather.6.cloned.1.call-start = ((), (), s32[]{:S(2)}) async-start(), calls=%async_computation.2 | async-start | bytes 2228224 | tf_op jit(solution)/shard_map/all_gather | solution.py:16
  546.1 147.8 %reduce-scatter.3.cloned.1.call-start = ((), (), s32[]{:S(2)}) async-start(), calls=%async_computation.4 | async-start | bytes 786432 | tf_op jit(solution)/shard_map/reduce_scatter | solution.py:176
  577.1 11.3 copy-start.26
  577.1 11.3 copy-start.16
  652.6 41.4 %copy-start.12 = (bf16[64,2048]{1,0:T(8,128)(2,1)S(1)}, bf16[64,2048]{1,0:T(8,128)(2,1)}, u32[]{:S(2)}) copy-start(bf16[64,2048]{1,0:T(8,128)(2,1)} %param.28) | copy-start | bytes 786436
  652.6 42.6 %copy-start.24 = (f32[2048]{0:T(1024)S(1)}, f32[2048]{0:T(1024)}, u32[]{:S(2)}) copy-start(f32[2048]{0:T(1024)} %param.29) | copy-start | bytes 24580
  652.6 186.6 %all-gather.10.cloned.1.call-start = ((), (), s32[]{:S(2)}) async-start(), calls=%async_computation.5 | async-start | bytes 12255232 | tf_op jit(solution)/shard_map/all_gather | solution.py:157
  653.2 328.2 %all-gather.12.cloned.1.call-start = ((), (), s32[]{:S(2)}) async-start(), calls=%async_computation.6 | async-start | bytes 12255232 | tf_op jit(solution)/shard_map/all_gather | solution.py:158
  653.7 510.5 %all-gather.14.cloned.1.call-start = ((), (), s32[]{:S(2)}) async-start(), calls=%async_computation.7 | async-start | bytes 12255232 | tf_op jit(solution)/shard_map/all_gather | solution.py:159
  654.3 529.8 %reduce-scatter.5.cloned.1.call-start = ((), (), s32[]{:S(2)}) async-start(), calls=%async_computation.8 | async-start | bytes 786432 | tf_op jit(solution)/shard_map/reduce_scatter | solution.py:204
  698.4 150.2 %copy-start.23 = (f32[3,2816]{1,0:T(4,128)S(1)}, f32[3,2816]{1,0:T(4,128)}, u32[]{:S(2)}) copy-start(f32[3,2816]{1,0:T(4,128)} %param.32) | copy-start | bytes 101380
  845.1 4.6 collective-permute-start
  1164.2 19.9 %copy-start.13 = (bf16[64,2048]{1,0:T(8,128)(2,1)S(1)}, bf16[64,2048]{1,0:T(8,128)(2,1)}, u32[]{:S(2)}) copy-start(bf16[64,2048]{1,0:T(8,128)(2,1)} %reduce-scatter.3.cloned.1.call-done) | copy-start | bytes 786436
  (32 other events, 70.3 us)
Sparse Core Ops, SparseCore 0:
  515.9 63.0 all-gather.7
  581.9 59.1 all-gather.5
  652.7 41.2 reduce-scatter.2
  696.6 142.5 all-gather.9
  841.7 139.5 all-gather.11
  983.9 180.2 all-gather.13
  1178.0 6.0 reduce-scatter.4
where the time goes:
time: 1210 us; the launch traced here: 1190 us
  waiting for transfers between devices  549 us (45%)
  matrix products  311 us (26%)
  local copies, waits for them, and re-layouts  248 us (20%)
  other arithmetic  64.1 us (5%)
  between operations  14.1 us (1%)
    all_gather x1, waiting for transfers between devices, body(): lax.all_gather(narrowing_projection, 'sp', axis=1, tiled=True)  183 us
    all_gather x1, waiting for transfers between devices, body(): lax.all_gather(switch_projection, 'sp', axis=0, tiled=True)  141 us
    all_gather x1, waiting for transfers between devices, body(): lax.all_gather(widening_projection, 'sp', axis=0, tiled=True)  130 us
    pad x8, local copies, waits for them, and re-layouts, recurrence(): lax.associative_scan(compose, (block_maps, block_states))  86 us
    dot_general x16, matrix products, span_step(): along = jnp.einsum('bhij,bhj->bhi', state, erase_dir, precision=highest)  79.9 us
    dot_general x16, matrix products, span_step(): jnp.einsum('bhij,bhj->bhi', state, acceptor_entries, precision=highest)  79 us
    dynamic_update_slice x32, local copies, waits for them, and re-layouts, recurrence(): lax.scan(span_step, (zero_state, start_maps), arranged)  57 us
    dot_general x16, matrix products, span_step(): jnp.einsum('bhij,bhj->bhi', mapping, erase_dir, precision=highest)  53.9 us
  transfers between devices with their start and end apart: 8, of which 7 were waited for; matrix products, arithmetic and copies ran while one was open for 7% of the time, Pallas kernels for 0%

commit v1 on v0

--- a/solution.py
+++ b/solution.py
@@ -153,10 +153,14 @@
     switch_filter_coefficients,
     narrowing_projection,
 ):
+
+    def mix_regions(m):
+        return jnp.concatenate(lax.all_gather(m, "sp"), axis=1)
+
     gate_full, up_full, down_full = (
         lax.all_gather(switch_projection, "sp", axis=0, tiled=True),
         lax.all_gather(widening_projection, "sp", axis=0, tiled=True),
-        lax.all_gather(narrowing_projection, "sp", axis=1, tiled=True),
+        mix_regions(narrowing_projection),
     )
     sublevel_arguments = mechanism_inputs(
         acceptor_signal, address_entries, payload_entries, fading_logits, learning_rate_logits

time: 1210 us -> 1170 us (0.967)
  waiting for transfers between devices: 549 us -> 494 us
  local copies, waits for them, and re-layouts: 248 us -> 263 us
    all_gather x1, waiting for transfers between devices: 183 us -> 133 us  [mix_regions(): return jnp.concatenate(lax.all_gather(m, 'sp'), axis=1)]
    reshape x0 -> x1, local copies, waits for them, and re-layouts: none -> 15.2 us  [mix_regions(): return jnp.concatenate(lax.all_gather(m, 'sp'), axis=1)]
  transfers between devices with their start and end apart: 8 -> 8, of which waited for: 7 -> 6; matrix products, arithmetic and copies ran while one was open for 7% -> 9% of each run, Pallas kernels for 0% -> 0%
where the time goes in v1:
time: 1170 us; the launch traced here: 1150 us
  waiting for transfers between devices  494 us (42%)
  matrix products  312 us (27%)
  local copies, waits for them, and re-layouts  263 us (22%)
  other arithmetic  64.1 us (5%)
  between operations  14.1 us (1%)
    all_gather x1, waiting for transfers between devices, body(): lax.all_gather(switch_projection, 'sp', axis=0, tiled=True)  141 us
    all_gather x1, waiting for transfers between devices, mix_regions(): return jnp.concatenate(lax.all_gather(m, 'sp'), axis=1)  133 us
    all_gather x1, waiting for transfers between devices, body(): lax.all_gather(widening_projection, 'sp', axis=0, tiled=True)  126 us
    pad x8, local copies, waits for them, and re-layouts, recurrence(): lax.associative_scan(compose, (block_maps, block_states))  85.3 us
    dot_general x16, matrix products, span_step(): along = jnp.einsum('bhij,bhj->bhi', state, erase_dir, precision=highest)  79.9 us
    dot_general x16, matrix products, span_step(): jnp.einsum('bhij,bhj->bhi', state, acceptor_entries, precision=highest)  79 us
    dynamic_update_slice x32, local copies, waits for them, and re-layouts, recurrence(): lax.scan(span_step, (zero_state, start_maps), arranged)  56.8 us
    dot_general x16, matrix products, span_step(): jnp.einsum('bhij,bhj->bhi', mapping, erase_dir, precision=highest)  53.9 us
  transfers between devices with their start and end apart: 8, of which 6 were waited for; matrix products, arithmetic and copies ran while one was open for 9% of the time, Pallas kernels for 0%

profile of v1, /device:TPU:0, one launch (start us, length us, event | category | flops | bytes accessed | tf_op | source)
XLA Modules:
  0.0 1152.8 jit_solution(1500716186759594818)
XLA Ops:
  23.2 417.7 %while.30 = (s32[]{:T(128)}, f32[8,8,64,64]{3,2,1,0:T(8,128)}, f32[8,8,64,64]{3,2,1,0:T(8,128)}, f32[16,8,8,64]{3,0,2,1:T(8,128)}, f32[16,8,8,64]{3,0,2,1:T(8,12...) while((s32[]{:T(128)}, f32[8,8,64,64]{3,2,1,0:T(8,128)}, ...), condition=%wide.region_2.3_spmd.clone, body=%wide.region_1.2_spmd.clone.sunk | while | flops 15204355 | bytes 25657612 | solution.py:125
  27.4 3.4 fusion.112
  41.0 4.9 convolution_bitcast_fusion.9
  48.5 5.1 fusion.113
  53.6 3.4 fusion.112
  67.2 4.9 convolution_bitcast_fusion.9
  74.7 5.1 fusion.113
  79.8 3.4 fusion.112
  93.4 4.9 convolution_bitcast_fusion.9
  100.9 5.1 fusion.113
  106.0 3.4 fusion.112
  119.7 4.9 convolution_bitcast_fusion.9
  127.1 5.1 fusion.113
  145.9 4.9 convolution_bitcast_fusion.9
  153.4 5.1 fusion.113
  172.1 4.9 convolution_bitcast_fusion.9
  179.6 5.1 fusion.113
  198.3 4.9 convolution_bitcast_fusion.9
  205.8 5.1 fusion.113
  224.5 4.9 convolution_bitcast_fusion.9
  232.0 5.1 fusion.113
  237.1 3.4 fusion.112
  250.7 4.9 convolution_bitcast_fusion.9
  258.2 5.1 fusion.113
  263.3 3.4 fusion.112
  276.9 4.9 convolution_bitcast_fusion.9
  284.4 5.1 fusion.113
  289.5 3.4 fusion.112
  303.1 4.9 convolution_bitcast_fusion.9
  310.6 5.1 fusion.113
  329.4 4.9 convolution_bitcast_fusion.9
  336.9 5.1 fusion.113
  342.0 3.4 fusion.112
  355.6 4.9 convolution_bitcast_fusion.9
  363.1 5.1 fusion.113
  368.2 3.4 fusion.112
  381.8 4.9 convolution_bitcast_fusion.9
  389.3 5.1 fusion.113
  408.0 4.9 convolution_bitcast_fusion.9
  415.5 5.1 fusion.113
  434.3 4.9 convolution_bitcast_fusion.9
  452.2 9.1 pad.48
  463.2 9.2 pad.47
  478.2 16.5 %pad.50 = f32[8,8,64,64]{3,2,1,0:T(8,128)} pad(f32[4,8,64,64]{3,2,1,0:T(8,128)} %copy-done.6, f32[]{:T(128)} %constant.54.clone.1), padding=1_0_1x0_0_0x0_0_0x0_0_0 | pad | bytes 1572868 | tf_op jit(solution)/shard_map/pad | solution.py:128
  497.0 16.6 %pad.49 = f32[8,8,64,64]{3,2,1,0:T(8,128)} pad(f32[4,8,64,64]{3,2,1,0:T(8,128)} %pad_maximum_fusion.1, f32[]{:T(128)} %constant.54.clone.1), padding=0_1_1x0_0_0x0_0_0x0_0_0 | pad | bytes 1572868 | tf_op jit(solution)/shard_map/pad | solution.py:128
  518.3 5.9 pad.41
  525.2 5.8 pad.42
  532.7 11.0 pad.112
  545.4 16.5 %pad.67 = f32[7,8,64,64]{3,2,1,0:T(8,128)} pad(f32[4,8,64,64]{3,2,1,0:T(8,128)} %pad_maximum_fusion.1, f32[]{:T(128)} %constant.54.clone.1), padding=0_0_1x0_0_0x0_0_0x0_0_0 | pad | bytes 1441796 | tf_op jit(solution)/shard_map/slice | solution.py:133
  562.8 11.1 pad.44
  576.0 11.1 pad.43
  588.2 4.0 slice_add_fusion.1
  593.7 46.9 %all-gather.7.cloned.1.call-done = bf16[16,8,64,64]{3,2,1,0:T(8,128)(2,1)} async-done(((bf16[1,8,64,64]{3,2,1,0:T(8,128)(2,1)}), bf16[16,8,64,64]{3,2,1,0:T(8,128)(2,1)}) %all-gather.7.cloned.1.call-update) | async-done | bytes 1048592 | tf_op jit(solution)/shard_map/all_gather | solution.py:16
  641.4 3.7 fusion.13
  645.1 3.4 fusion.69
  653.9 39.6 %reduce-scatter.3.cloned.1.call-done = bf16[64,2048]{1,0:T(8,128)(2,1)} async-done(((bf16[128,2048]{1,0:T(8,128)(2,1)}), bf16[64,2048]{1,0:T(8,128)(2,1)}) %reduce-scatter.3.cloned.1.call-update) | async-done | bytes 262160 | tf_op jit(solution)/shard_map/reduce_scatter | solution.py:180
  697.9 140.8 %all-gather.11.cloned.1.call-done = bf16[2048,2816]{1,0:T(8,128)(2,1)} async-done(((bf16[128,2816]{1,0:T(8,128)(2,1)}), bf16[2048,2816]{1,0:T(8,128)(2,1)}) %all-gather.11.cloned.1.call-update) | async-done | bytes 11534352 | tf_op jit(solution)/shard_map/all_gather | solution.py:161
  838.6 5.9 convolution_convert_fusion.1
  844.6 3.4 collective-permute-start
  848.2 132.7 %all-gather.15.cloned.1.call-done = bf16[45056,128]{1,0:T(8,128)(2,1)} async-done(((bf16[2816,128]{1,0:T(8,128)(2,1)}), bf16[45056,128]{1,0:T(8,128)(2,1)}) %all-gather.15.cloned.1.call-update) | async-done | bytes 11534352 | tf_op jit(solution)/shard_map/all_gather | solution.py:158
  980.9 15.2 %copy.92 = bf16[2816,16,128]{0,2,1:T(8,128)(2,1)} copy(bf16[2816,16,128]{2,0,1:T(8,128)(2,1)} %bitcast.190) | data formatting | bytes 23068672 | tf_op jit(solution)/shard_map/reshape | solution.py:158
  997.5 125.7 %all-gather.13.cloned.1.call-done = bf16[2048,2816]{1,0:T(8,128)(2,1)} async-done(((bf16[128,2816]{1,0:T(8,128)(2,1)}), bf16[2048,2816]{1,0:T(8,128)(2,1)}) %all-gather.13.cloned.1.call-update) | async-done | bytes 11534352 | tf_op jit(solution)/shard_map/all_gather | solution.py:162
  1123.1 14.8 %convolution_convert_fusion.2 = bf16[128,2048]{1,0:T(8,128)(2,1)} fusion(bf16[2816,2048]{0,1:T(8,128)(2,1)} %bitcast.191, bf16[128,2048]{1,0:T(8,128)(2,1)S(1)} %all_gather.25, bf16[2048,2816]{1,0:T(8,128)(2,1)} %all-gather.13.cloned.1.call-done, f32[130,2816]{1,0:T(8,128)} %maximum_convert_fusion, f32[2816]{0:T(1024)S(1)} %get-tuple-element.204, ...), kind=kOutput, calls=%fused_computation.27 | convolution fusion | flops 2957737984 | bytes 28476416 | tf_op jit(solution)/shard_map/dot_general | solution.py:209
  1137.9 6.3 reduce-scatter.5.cloned.1.call-done
  (389 shorter events, 297.2 us)
Async XLA Ops:
  6.5 643.3 %copy-start = (bf16[512,2048]{1,0:T(8,128)(2,1)S(1)}, bf16[512,2048]{1,0:T(8,128)(2,1)}, u32[]{:S(2)}) copy-start(bf16[512,2048]{1,0:T(8,128)(2,1)} %param.27) | copy-start | bytes 6291460
  6.5 587.1 %all-gather.9.cloned.1.call-start = ((), (), s32[]{:S(2)}) async-start(), calls=%async_computation.3 | async-start | bytes 2228224 | tf_op jit(solution)/shard_map/all_gather | solution.py:16
  7.9 13.7 %copy-start.22 = (f32[64,64]{1,0:T(8,128)}, f32[64,64]{1,0:T(8,128)S(1)}, u32[]{:S(2)}) copy-start(f32[64,64]{1,0:T(8,128)S(1)} %fusion.61) | copy-start | bytes 49156
  12.0 9.6 copy-start.16
  24.0 8.3 copy-start.4
  34.5 4.7 copy-start.5
  48.5 5.1 copy-start.1
  48.5 10.0 copy-start.4
  60.7 4.7 copy-start.5
  74.7 5.1 copy-start.1
  74.7 10.0 copy-start.4
  86.9 4.7 copy-start.5
  100.9 5.1 copy-start.1
  100.9 10.0 copy-start.4
  113.1 4.7 copy-start.5
  127.1 5.1 copy-start.1
  127.1 10.0 copy-start.4
  139.4 4.7 copy-start.5
  153.3 5.1 copy-start.1
  153.3 10.0 copy-start.4
  165.6 4.7 copy-start.5
  179.6 5.1 copy-start.1
  179.6 10.0 copy-start.4
  191.8 4.7 copy-start.5
  205.8 5.1 copy-start.1
  205.8 10.0 copy-start.4
  218.0 4.7 copy-start.5
  232.0 5.1 copy-start.1
  232.0 10.0 copy-start.4
  244.2 4.7 copy-start.5
  258.2 5.1 copy-start.1
  258.2 10.0 copy-start.4
  270.4 4.7 copy-start.5
  284.4 5.1 copy-start.1
  284.4 10.0 copy-start.4
  296.6 4.7 copy-start.5
  310.6 5.1 copy-start.1
  310.6 10.0 copy-start.4
  322.8 4.7 copy-start.5
  336.9 5.1 copy-start.1
  336.9 10.0 copy-start.4
  349.1 4.7 copy-start.5
  363.1 5.1 copy-start.1
  363.1 10.0 copy-start.4
  389.3 5.1 copy-start.1
  389.3 10.0 copy-start.4
  415.5 5.1 copy-start.1
  415.5 10.0 copy-start.4
  450.4 10.9 slice-start
  478.2 16.5 %copy-start.18 = (f32[1,8,64,64]{3,2,1,0:T(8,128)S(1)}, f32[1,8,64,64]{3,2,1,0:T(8,128)}, u32[]{:S(2)}) copy-start(f32[1,8,64,64]{3,2,1,0:T(8,128)} %slice.129) | copy-start | bytes 393220
  515.3 125.3 %all-gather.7.cloned.1.call-start = ((), (), s32[]{:S(2)}) async-start(), calls=%async_computation.2 | async-start | bytes 2228224 | tf_op jit(solution)/shard_map/all_gather | solution.py:16
  545.3 148.1 %reduce-scatter.3.cloned.1.call-start = ((), (), s32[]{:S(2)}) async-start(), calls=%async_computation.4 | async-start | bytes 786432 | tf_op jit(solution)/shard_map/reduce_scatter | solution.py:180
  576.0 11.1 copy-start.27
  576.0 11.2 copy-start.17
  652.1 41.4 %copy-start.12 = (bf16[64,2048]{1,0:T(8,128)(2,1)S(1)}, bf16[64,2048]{1,0:T(8,128)(2,1)}, u32[]{:S(2)}) copy-start(bf16[64,2048]{1,0:T(8,128)(2,1)} %param.28) | copy-start | bytes 786436
  652.1 42.6 %copy-start.25 = (f32[2048]{0:T(1024)S(1)}, f32[2048]{0:T(1024)}, u32[]{:S(2)}) copy-start(f32[2048]{0:T(1024)} %param.29) | copy-start | bytes 24580
  652.1 186.6 %all-gather.11.cloned.1.call-start = ((), (), s32[]{:S(2)}) async-start(), calls=%async_computation.5 | async-start | bytes 12255232 | tf_op jit(solution)/shard_map/all_gather | solution.py:161
  652.7 328.2 %all-gather.15.cloned.1.call-start = ((), (), s32[]{:S(2)}) async-start(), calls=%async_computation.8 | async-start | bytes 12255232 | tf_op jit(solution)/shard_map/all_gather | solution.py:158
  653.2 469.9 %all-gather.13.cloned.1.call-start = ((), (), s32[]{:S(2)}) async-start(), calls=%async_computation.6 | async-start | bytes 12255232 | tf_op jit(solution)/shard_map/all_gather | solution.py:162
  653.8 490.4 %reduce-scatter.5.cloned.1.call-start = ((), (), s32[]{:S(2)}) async-start(), calls=%async_computation.7 | async-start | bytes 786432 | tf_op jit(solution)/shard_map/reduce_scatter | solution.py:208
  697.9 150.2 %copy-start.24 = (f32[3,2816]{1,0:T(4,128)S(1)}, f32[3,2816]{1,0:T(4,128)}, u32[]{:S(2)}) copy-start(f32[3,2816]{1,0:T(4,128)} %param.32) | copy-start | bytes 101380
  844.6 151.5 %collective-permute-start = (bf16[2,2816]{1,0:T(2,128)(2,1)S(1)}, bf16[2,2816]{1,0:T(2,128)(2,1)S(1)}, u32[]{:S(2)}, u32[]{:S(2)}) collective-permute-start(bf16[2,2816]{1,0:T(2,128)(2,1)S(1)} %slice.166), channel_id=1, source_target_pairs={{0,2},{2,4},{4,6},{6,8},{8,10},{10,12},{12,14},{14,16},{16,18},{18... | collective-permute-start | bytes 33800 | tf_op jit(solution)/shard_map/ppermute | solution.py:36
  1123.1 21.1 %copy-start.13 = (bf16[64,2048]{1,0:T(8,128)(2,1)S(1)}, bf16[64,2048]{1,0:T(8,128)(2,1)}, u32[]{:S(2)}) copy-start(bf16[64,2048]{1,0:T(8,128)(2,1)} %param.28) | copy-start | bytes 786436
  1123.1 21.1 %copy-start.14 = (bf16[64,2048]{1,0:T(8,128)(2,1)S(1)}, bf16[64,2048]{1,0:T(8,128)(2,1)}, u32[]{:S(2)}) copy-start(bf16[64,2048]{1,0:T(8,128)(2,1)} %reduce-scatter.3.cloned.1.call-done) | copy-start | bytes 786436
  (33 other events, 75.0 us)
Sparse Core Ops, SparseCore 0:
  515.4 63.0 all-gather.8
  581.3 59.1 all-gather.6
  652.2 41.2 reduce-scatter.2
  696.1 142.5 all-gather.10
  841.2 139.5 all-gather.14
  983.5 139.5 all-gather.12
  1138.0 6.1 reduce-scatter.4
